TPU v7x, 32 devices: a whole 2x2x4 slice. The times are simulated.
32 devices in a mesh: gr: 2 (over x), fs: 8 (over z, y), tp: 2 (over core).
Axes of the slice: x: 2, y: 2, z: 4, core: 2. Of those that a mesh axis runs over, the one named last changes fastest.
Arguments:
- tokens: bfloat16 [4096, 2048], P(('gr', 'fs', 'tp')), may hold values from -6 to 6
- routes: int32 [4096, 8], P(('gr', 'fs', 'tp')), may hold values from 0 to 15, all different within a row; in each aligned block of 128 rows (0 to 127, 128 to 255, ...) at most 96 rows name the same one
- route_weights: float32 [4096, 8], P(('gr', 'fs', 'tp')), may hold values from 0.1 to 0.6
- norm_gain: float32 [2048], P(('gr', 'tp')), may hold values from 0.1 to 1.9
- gate_trained: float32 [16, 384, 2048], P(None, 'fs', ('gr', 'tp')), may hold values from -0.125 to 0.125
- up_trained: float32 [16, 384, 2048], P(None, 'fs', ('gr', 'tp')), may hold values from -0.125 to 0.125
- down_trained: float32 [16, 384, 2048], P(None, 'fs', ('gr', 'tp')), may hold values from -0.3125 to 0.3125
- shared_gate_trained: float32 [512, 2048], P('fs', ('gr', 'tp')), may hold values from -0.125 to 0.125
- shared_up_trained: float32 [512, 2048], P('fs', ('gr', 'tp')), may hold values from -0.125 to 0.125
- shared_down_trained: float32 [512, 2048], P('fs', ('gr', 'tp')), may hold values from -0.25 to 0.25
Outputs:
- combined: bfloat16 [4096, 2048], P(('gr', 'fs', 'tp'))
- expert_gate: bfloat16 [16, 384, 2048], P(('fs', 'tp'))
- expert_up: bfloat16 [16, 384, 2048], P(('fs', 'tp'))
- expert_down: bfloat16 [16, 384, 2048], P(('fs', 'tp'))
- shared_gate: bfloat16 [512, 2048], P('fs')
- shared_up: bfloat16 [512, 2048], P('fs')
- shared_down: bfloat16 [512, 2048], P('fs')
Inputs may be any that keep to these rules, and one draw needn't show every extreme that they name: `routes`: each row names 8 different experts. Among the rows of one device no expert is named more than 96 times, and that many is reached in every draw.
All inputs are finite; a program needn't handle non-finite values.
Results may differ from a plain program's by a relative error of at most 0.0084.
Values may be sent and summed in bfloat16 or wider, within the bound.
A program may use at most 128 MiB of HBM per device.

v0:
```python
import jax
import jax.numpy as jnp
from jax import lax
from jax.sharding import PartitionSpec as P

epsilon = 1e-06


def contract_rows(inputs, matrix):
    return lax.dot_general(
        inputs, matrix, (((1,), (1,)), ((), ())), preferred_element_type=jnp.float32
    )


def swiglu_rows(inputs, gate_matrix, up_matrix, down_matrix):
    hidden = (
        jax.nn.silu(contract_rows(inputs, gate_matrix)) * contract_rows(inputs, up_matrix)
    ).astype(jnp.bfloat16)
    return jnp.dot(hidden, down_matrix, preferred_element_type=jnp.float32)


def body(
    tokens,
    routes,
    route_weights,
    norm_gain,
    gate_trained,
    up_trained,
    down_trained,
    shared_gate_trained,
    shared_up_trained,
    shared_down_trained,
):
    gain_row = norm_gain[None, None, :]
    stacked = jnp.stack(
        [gate_trained * gain_row, up_trained * gain_row, down_trained], axis=1
    ).astype(jnp.bfloat16)
    halves = lax.all_to_all(
        lax.all_to_all(stacked[:, :, :, None, :], "fs", split_axis=0, concat_axis=2, tiled=True),
        "tp",
        split_axis=0,
        concat_axis=3,
        tiled=True,
    )
    owned = lax.all_gather(halves[:, :, :, None], "gr", axis=3, tiled=True)
    owned = owned.reshape(owned.shape[0], 3, owned.shape[2], -1)
    expert_gate = owned[:, 0]
    expert_up = owned[:, 1]
    expert_down = owned[:, 2]
    shared_gain = norm_gain[None, :]
    shared_stack = jnp.stack(
        [shared_gate_trained * shared_gain, shared_up_trained * shared_gain, shared_down_trained],
        axis=0,
    ).astype(jnp.bfloat16)
    shared_whole = lax.all_gather(shared_stack, ("gr", "tp"), axis=2, tiled=True)
    shared_gate = shared_whole[0]
    shared_up = shared_whole[1]
    shared_down = shared_whole[2]
    values = tokens.astype(jnp.float32)
    normed = (
        values * lax.rsqrt(jnp.mean(values * values, axis=1, keepdims=True) + epsilon)
    ).astype(jnp.bfloat16)
    row_count, features = normed.shape
    per_token = routes.shape[1]
    shared_out = swiglu_rows(
        normed,
        lax.all_gather(shared_gate, "fs", axis=0, tiled=True),
        lax.all_gather(shared_up, "fs", axis=0, tiled=True),
        lax.all_gather(shared_down, "fs", axis=0, tiled=True),
    )
    experts = lax.axis_size("fs") * lax.axis_size("tp")
    capacity = max(2, 3 * row_count * per_token // (2 * experts))
    chosen = routes.reshape(-1)
    onehot = (chosen[:, None] == jnp.arange(experts, dtype=jnp.int32)[None, :]).astype(jnp.int32)
    position = jnp.sum((jnp.cumsum(onehot, axis=0) - onehot) * onehot, axis=1)
    target = chosen * capacity + position
    source = (
        jnp.full((experts * capacity,), row_count, jnp.int32)
        .at[target]
        .set(jnp.arange(row_count * per_token, dtype=jnp.int32) // per_token)
    )
    padded = jnp.concatenate([normed, jnp.zeros((1, features), jnp.bfloat16)], axis=0)
    outgoing = padded[source].reshape(experts, capacity, features)
    arrived = lax.all_to_all(outgoing, ("fs", "tp"), split_axis=0, concat_axis=0, tiled=True)
    item_count = arrived.shape[1]
    result = swiglu_rows(
        arrived.reshape(-1, features), expert_gate[0], expert_up[0], expert_down[0]
    )
    result = result.astype(jnp.bfloat16).reshape(experts, item_count, features)
    returned = lax.all_to_all(result, ("fs", "tp"), split_axis=0, concat_axis=0, tiled=True)
    picked = returned.reshape(experts * capacity, features)[target].astype(jnp.float32)
    picked = picked.reshape(row_count, per_token, features)
    routed = jnp.sum(picked * route_weights[:, :, None], axis=1)
    combined = (routed + shared_out).astype(jnp.bfloat16)
    return (combined, expert_gate, expert_up, expert_down, shared_gate, shared_up, shared_down)


def solution(mesh):
    in_specs = (
        P(("gr", "fs", "tp"), None),
        P(("gr", "fs", "tp"), None),
        P(("gr", "fs", "tp"), None),
        P(("gr", "tp")),
        P(None, "fs", ("gr", "tp")),
        P(None, "fs", ("gr", "tp")),
        P(None, "fs", ("gr", "tp")),
        P("fs", ("gr", "tp")),
        P("fs", ("gr", "tp")),
        P("fs", ("gr", "tp")),
    )
    out_specs = (
        P(("gr", "fs", "tp"), None),
        P(("fs", "tp"), None, None),
        P(("fs", "tp"), None, None),
        P(("fs", "tp"), None, None),
        P("fs", None),
        P("fs", None),
        P("fs", None),
    )
    return jax.shard_map(body, mesh=mesh, in_specs=in_specs, out_specs=out_specs, check_vma=False)
```

profile of v0, /device:TPU:0, one launch (start us, length us, event | category | flops | bytes accessed | tf_op | source)
XLA Modules:
  0.0 506.6 jit_solution(6187070013755928364)
XLA Ops:
  8.0 1.6 convert_bitcast_fusion
  9.7 0.2 copy-done.1
  9.9 1.9 fusion.27
  11.8 1.7 pad_maximum_fusion
  13.5 7.4 %all-to-all-start.1 = ((bf16[16,3,48,1,512]{4,2,3,1,0:T(8,128)(2,1)}), bf16[16,3,48,1,512]{4,2,3,1,0:T(8,128)(2,1)S(1)}, u32[]{:S(2)}, u32[]{:S(2)}) async-start(bf16[16,3,48,1,512]{4,2,3,1,0:T(8,128)(2,1)} %pad_maximum_fusion), calls=%async_computation.1 | async-start | bytes 4718592 | tf_op jit(solution)/shard_map/all_to_all | solution.py:39
  20.9 0.1 copy.38
  21.0 0.1 eq.29
  21.1 0.1 eq.25
  21.2 4.5 reduce-window.6
  25.8 0.1 slice.36
  25.8 0.1 copy.40
  26.0 0.1 copy.41
  26.1 0.1 copy.37
  26.2 0.1 mul.85
  26.3 0.2 fusion.23
  26.5 0.2 fusion.24
  26.7 0.1 broadcast_add_fusion
  26.9 4.3 scatter_custom_fusion
  31.2 7.1 %gather_fusion = bf16[1536,2048]{1,0:T(8,128)(2,1)} fusion(bf16[129,2048]{1,0:T(8,128)(2,1)S(1)} %concatenate.11, s32[2048]{0:T(1024)S(1)} %pad_clamp_fusion), kind=kCustom, calls=%fused_computation | custom fusion | bytes 12589056 | tf_op jit(solution)/shard_map/gather | solution.py:83
  38.3 36.5 %all-to-all-done.1 = bf16[16,3,48,1,512]{4,2,3,1,0:T(8,128)(2,1)S(1)} async-done(((bf16[16,3,48,1,512]{4,2,3,1,0:T(8,128)(2,1)}), bf16[16,3,48,1,512]{4,2,3,1,0:T(8,128)(2,1)S(1)}, u32[]{:S(2)}, u32[]{:S(2)}) %all-to-all-start.1) | async-done | bytes 2359328 | tf_op jit(solution)/shard_map/all_to_all | solution.py:39
  74.8 0.2 copy.43
  74.9 6.5 %all_to_all.43 = bf16[2,3,384,1,512]{4,2,1,3,0:T(8,128)(2,1)} all-to-all(bf16[2,3,384,1,512]{4,2,1,3,0:T(8,128)(2,1)S(1)} %bitcast.99), channel_id=1, replica_groups=mesh['gr'=2,'fs'=8,'tp'=2] {'tp'}, dimensions={0} | all-to-all | bytes 4718592 | tf_op jit(solution)/shard_map/all_to_all | solution.py:38
  81.5 4.7 all-to-all-start
  86.2 0.7 all-gather.9.cloned.1.call-update
  86.9 65.5 %all-gather.9.cloned.1.call-done = bf16[1,3,384,4,1,512]{5,2,4,1,0,3:T(8,128)(2,1)} async-done(((bf16[1,3,384,2,1,512]{5,2,4,1,0,3:T(8,128)(2,1)}), bf16[1,3,384,4,1,512]{5,2,4,1,0,3:T(8,128)(2,1)}) %all-gather.9.cloned.1.call-update) | async-done | bytes 4718608 | tf_op jit(solution)/shard_map/all_gather | solution.py:45
  152.4 6.6 %copy.45 = bf16[1,3,384,4,1,512]{2,5,3,1,4,0:T(8,128)(2,1)} copy(bf16[1,3,384,4,1,512]{5,2,4,1,0,3:T(8,128)(2,1)} %all-gather.9.cloned.1.call-done) | data formatting | bytes 9437184 | tf_op jit(solution)/shard_map/all_gather | solution.py:45
  159.0 41.1 %all-to-all-done = bf16[16,96,2048]{2,1,0:T(8,128)(2,1)} async-done(((bf16[16,96,2048]{2,1,0:T(8,128)(2,1)}), bf16[16,96,2048]{2,1,0:T(8,128)(2,1)}, u32[]{:S(2)}, u32[]{:S(2)}) %all-to-all-start) | async-done | bytes 6291488 | tf_op jit(solution)/shard_map/all_to_all | solution.py:84
  200.2 5.9 %fusion.10 = f32[1536,384]{1,0:T(8,128)S(1)} fusion(bf16[1536,2048]{1,0:T(8,128)(2,1)} %bitcast.5, bf16[1,3,384,2048]{2,3,1,0:T(8,128)(2,1)} %bitcast.94), kind=kOutput, calls=%fused_computation.18 | convolution fusion | flops 2415919104 | bytes 10223616 | tf_op jit(solution)/shard_map/dot_general | solution.py:10
  206.1 11.4 %convolution_convert_fusion = bf16[1536,2048]{1,0:T(8,128)(2,1)} fusion(bf16[1,3,384,2048]{2,3,1,0:T(8,128)(2,1)} %bitcast.95, bf16[1536,2048]{1,0:T(8,128)(2,1)} %bitcast.5, f32[1536,384]{1,0:T(8,128)S(1)} %fusion.10), kind=kOutput, calls=%fused_computation.5 | convolution fusion | flops 4838522880 | bytes 18087936 | tf_op jit(solution)/shard_map/dot_general | solution.py:19
  217.5 28.2 %all-to-all-start.3 = ((bf16[16,96,2048]{2,1,0:T(8,128)(2,1)}), bf16[16,96,2048]{2,1,0:T(8,128)(2,1)}, u32[]{:S(2)}, u32[]{:S(2)}) async-start(bf16[16,96,2048]{2,1,0:T(8,128)(2,1)} %bitcast.100), calls=%async_computation.3 | async-start | bytes 12582912 | tf_op jit(solution)/shard_map/all_to_all | solution.py:90
  245.9 8.7 %all_gather.16 = bf16[3,64,2048]{2,1,0:T(8,128)(2,1)S(1)} all-gather(bf16[3,64,512]{2,1,0:T(8,128)(2,1)S(1)} %pad_maximum_fusion.1), channel_id=1, replica_groups=mesh['gr'=2,'fs'=8,'tp'=2] {'gr','tp'}, dimensions={2}, use_global_device_ids=true | all-gather | bytes 983040 | tf_op jit(solution)/shard_map/all_gather | solution.py:55
  254.6 1.2 slice_bitcast_fusion.3
  255.9 0.5 all-gather.13.cloned.1.call-update
  256.4 0.2 all-gather.15.cloned.1.call-start
  256.7 0.3 all-gather.15.cloned.1.call-update
  257.0 0.1 copy.46
  257.1 111.5 %all-gather.11.cloned.1.call-done = bf16[1,512,2048]{2,1,0:T(8,128)(2,1)} async-done(((bf16[1,64,2048]{2,1,0:T(8,128)(2,1)}), bf16[1,512,2048]{2,1,0:T(8,128)(2,1)}) %all-gather.11.cloned.1.call-update) | async-done | bytes 2097168 | tf_op jit(solution)/shard_map/all_gather | solution.py:67
  368.6 2.4 fusion.6
  371.0 4.5 slice_bitcast_fusion
  375.5 2.6 copy.47
  378.1 2.6 copy.48
  380.7 1.6 copy.49
  382.3 2.8 all-to-all-done.3
  385.1 12.4 %gather_fusion.1 = bf16[1024,2048]{1,0:T(8,128)(2,1)} fusion(bf16[1536,2048]{1,0:T(8,128)(2,1)} %bitcast.21, s32[1024]{0:T(1024)S(1)} %broadcast_clamp_fusion), kind=kCustom, calls=%fused_computation.1 | custom fusion | bytes 8392704 | tf_op jit(solution)/shard_map/gather | solution.py:91
  397.5 6.5 %fusion = f32[128,2048]{1,0:T(8,128)S(1)} fusion(bf16[1024,2048]{1,0:T(8,128)(2,1)} %gather_fusion.1, f32[128,8]{1,0:T(8,128)S(1)} %copy.46), kind=kLoop, calls=%fused_computation.4 | loop fusion | flops 6029312 | bytes 5246976 | tf_op jit(solution)/shard_map/reduce_sum | solution.py:93
  404.0 40.6 %all-gather.13.cloned.1.call-done = bf16[1,512,2048]{2,1,0:T(8,128)(2,1)} async-done(((bf16[1,64,2048]{2,1,0:T(8,128)(2,1)}), bf16[1,512,2048]{2,1,0:T(8,128)(2,1)}) %all-gather.13.cloned.1.call-update) | async-done | bytes 2097168 | tf_op jit(solution)/shard_map/all_gather | solution.py:68
  444.6 50.2 %all-gather.15.cloned.1.call-done = bf16[1,512,2048]{2,1,0:T(8,128)(2,1)} async-done(((bf16[1,64,2048]{2,1,0:T(8,128)(2,1)}), bf16[1,512,2048]{2,1,0:T(8,128)(2,1)}) %all-gather.15.cloned.1.call-update) | async-done | bytes 2097168 | tf_op jit(solution)/shard_map/all_gather | solution.py:69
  494.7 4.3 fusion.2
  (34 shorter events, 0.4 us)
Async XLA Ops:
  8.0 1.7 copy-start.6
  8.0 1.9 copy-start.1
  13.5 7.4 %copy-start.5 = (s32[128,8]{0,1:T(8,128)S(1)}, s32[128,8]{0,1:T(8,128)}, u32[]{:S(2)}) copy-start(s32[128,8]{0,1:T(8,128)} %param.11) | copy-start | bytes 12292
  13.5 12.8 %copy-start = (bf16[128,2048]{1,0:T(8,128)(2,1)S(1)}, bf16[128,2048]{1,0:T(8,128)(2,1)}, u32[]{:S(2)}) copy-start(bf16[128,2048]{1,0:T(8,128)(2,1)} %param.10) | copy-start | bytes 1572868
  13.5 61.3 %all-to-all-start.1 = ((bf16[16,3,48,1,512]{4,2,3,1,0:T(8,128)(2,1)}), bf16[16,3,48,1,512]{4,2,3,1,0:T(8,128)(2,1)S(1)}, u32[]{:S(2)}, u32[]{:S(2)}) async-start(bf16[16,3,48,1,512]{4,2,3,1,0:T(8,128)(2,1)} %pad_maximum_fusion), calls=%async_computation.1 | async-start | bytes 4718592 | tf_op jit(solution)/shard_map/all_to_all | solution.py:39
  81.5 118.7 %all-to-all-start = ((bf16[16,96,2048]{2,1,0:T(8,128)(2,1)}), bf16[16,96,2048]{2,1,0:T(8,128)(2,1)}, u32[]{:S(2)}, u32[]{:S(2)}) async-start(bf16[16,96,2048]{2,1,0:T(8,128)(2,1)} %bitcast.93), calls=%async_computation | async-start | bytes 12582912 | tf_op jit(solution)/shard_map/all_to_all | solution.py:84
  86.2 66.2 %all-gather.9.cloned.1.call-start = ((), (), s32[]{:S(2)}) async-start(), calls=%async_computation.4 | async-start | bytes 7077888 | tf_op jit(solution)/shard_map/all_gather | solution.py:45
  217.5 28.3 %copy-start.4 = (f32[64,512]{1,0:T(8,128)S(1)}, f32[64,512]{1,0:T(8,128)}, u32[]{:S(2)}) copy-start(f32[64,512]{1,0:T(8,128)} %param.19) | copy-start | bytes 393220
  217.5 28.3 %copy-start.2 = (f32[64,512]{1,0:T(8,128)S(1)}, f32[64,512]{1,0:T(8,128)}, u32[]{:S(2)}) copy-start(f32[64,512]{1,0:T(8,128)} %param.17) | copy-start | bytes 393220
  217.5 28.3 %copy-start.3 = (f32[64,512]{1,0:T(8,128)S(1)}, f32[64,512]{1,0:T(8,128)}, u32[]{:S(2)}) copy-start(f32[64,512]{1,0:T(8,128)} %param.18) | copy-start | bytes 393220
  217.5 167.6 %all-to-all-start.3 = ((bf16[16,96,2048]{2,1,0:T(8,128)(2,1)}), bf16[16,96,2048]{2,1,0:T(8,128)(2,1)}, u32[]{:S(2)}, u32[]{:S(2)}) async-start(bf16[16,96,2048]{2,1,0:T(8,128)(2,1)} %bitcast.100), calls=%async_computation.3 | async-start | bytes 12582912 | tf_op jit(solution)/shard_map/all_to_all | solution.py:90
  245.7 122.9 %all-gather.11.cloned.1.call-start = ((), (), s32[]{:S(2)}) async-start(), calls=%async_computation.5 | async-start | bytes 2359296 | tf_op jit(solution)/shard_map/all_gather | solution.py:67
  245.9 11.2 %copy-start.7 = (f32[128,8]{0,1:T(8,128)S(1)}, f32[128,8]{0,1:T(8,128)}, u32[]{:S(2)}) copy-start(f32[128,8]{0,1:T(8,128)} %param.12) | copy-start | bytes 12292
  255.8 188.7 %all-gather.13.cloned.1.call-start = ((), (), s32[]{:S(2)}) async-start(), calls=%async_computation.6 | async-start | bytes 2359296 | tf_op jit(solution)/shard_map/all_gather | solution.py:68
  256.4 238.3 %all-gather.15.cloned.1.call-start = ((), (), s32[]{:S(2)}) async-start(), calls=%async_computation.7 | async-start | bytes 2359296 | tf_op jit(solution)/shard_map/all_gather | solution.py:69
Sparse Core Ops, SparseCore 0:
  88.5 63.8 all-gather.8
Sparse Core Ops, SparseCore 1:
  255.9 112.6 all-gather.10
  370.6 73.9 all-gather.12
  447.1 47.5 all-gather.14
where the time goes:
time: 507 us
  waiting for transfers between devices  350 us (69%)
  local copies, waits for them, and re-layouts  44.2 us (9%)
  starting transfers between devices  40.7 us (8%)
  matrix products  24 us (5%)
  other arithmetic  16.8 us (3%)
  between operations  15.9 us (3%)
  blocking collectives  15.2 us (3%)
    all_gather x1, waiting for transfers between devices, body(): lax.all_gather(shared_gate, 'fs', axis=0, tiled=True)  111 us
    all_gather x1, waiting for transfers between devices, body(): owned = lax.all_gather(halves[:, :, :, None], 'gr', axis=3, tiled=True)  65.5 us
    all_gather x1, waiting for transfers between devices, body(): lax.all_gather(shared_down, 'fs', axis=0, tiled=True)  50.2 us
    all_to_all x1, waiting for transfers between devices, body(): lax.all_to_all(outgoing, ('fs', 'tp'), split_axis=0, concat_axis=0, tiled...  41.1 us
    all_gather x1, waiting for transfers between devices, body(): lax.all_gather(shared_up, 'fs', axis=0, tiled=True)  40.6 us
    all_to_all x1, waiting for transfers between devices, body(): lax.all_to_all(stacked[:, :, :, None, :], 'fs', split_axis=0, concat_axis...  36.5 us
    all_to_all x1, starting transfers between devices, body(): lax.all_to_all(result, ('fs', 'tp'), split_axis=0, concat_axis=0, tiled=T...  28.2 us
    dot_general x2, matrix products, swiglu_rows(): return jnp.dot(hidden, down_matrix, preferred_element_type=jnp.float32)  15.6 us
  transfers between devices with their start and end apart: 7, of which 7 were waited for; matrix products, arithmetic and copies ran while one was open for 11% of the time, Pallas kernels for 0%

commit v1 on v0

--- a/solution.py
+++ b/solution.py
@@ -1,9 +1,15 @@
+import functools
+
 import jax
 import jax.numpy as jnp
 from jax import lax
+from jax.experimental import pallas as pl
+from jax.experimental.pallas import tpu as pltpu
 from jax.sharding import PartitionSpec as P
 
 epsilon = 1e-06
+LANES = 128
+MESH = pl.DeviceIdType.MESH
 
 
 def contract_rows(inputs, matrix):
@@ -19,7 +25,7 @@
     return jnp.dot(hidden, down_matrix, preferred_element_type=jnp.float32)
 
 
-def body(
+def dispatch_body(
     tokens,
     routes,
     route_weights,
@@ -95,6 +101,392 @@
     return (combined, expert_gate, expert_up, expert_down, shared_gate, shared_up, shared_down)
 
 
+def exchange_kernel(
+    n,
+    pieces_ref,
+    shared_ref,
+    rows_ref,
+    combined_ref,
+    gate_ref,
+    up_ref,
+    down_ref,
+    shared_gate_ref,
+    shared_up_ref,
+    shared_down_ref,
+    weights,
+    shared,
+    rows,
+    parts,
+    pair_in,
+    sums,
+    sums_in,
+    local_sem,
+    piece_sem,
+    weight_sem,
+    column_out_sem,
+    column_sem,
+    shared_out_sem,
+    shared_sem,
+    row_out_sem,
+    row_sem,
+    row_pair_out_sem,
+    row_pair_sem,
+    part_sem,
+    part_recv_sem,
+    sum_sem,
+    sum_recv_sem,
+    out_sem,
+):
+    gr, fs, tp = lax.axis_index("gr"), lax.axis_index("fs"), lax.axis_index("tp")
+    other = 1 - tp
+    across = (1 - gr, fs, tp)
+    twin = (gr, fs, other)
+    expert = fs * 2 + tp
+    hidden_piece, width = pieces_ref.shape[2], pieces_ref.shape[3]
+    hidden = n * hidden_piece
+    shared_piece = shared_ref.shape[1]
+    extra = shared_piece // 2
+    features = 4 * width
+    row_count = rows_ref.shape[0]
+
+    barrier = pltpu.get_barrier_semaphore()
+    pl.semaphore_signal(barrier, inc=1, device_id=across, device_id_type=MESH)
+    pl.semaphore_signal(barrier, inc=1, device_id=twin, device_id_type=MESH)
+    for k in range(1, n):
+        for t in range(2):
+            pl.semaphore_signal(
+                barrier, inc=1, device_id=(gr, lax.rem(fs + k, n), t), device_id_type=MESH
+            )
+    pl.semaphore_wait(barrier, 2 * n)
+
+    def remote(src, dst, send, recv, device):
+        return pltpu.make_async_remote_copy(
+            src_ref=src,
+            dst_ref=dst,
+            send_sem=send,
+            recv_sem=recv,
+            device_id=device,
+            device_id_type=MESH,
+        )
+
+    def columns(g, t):
+        return pl.ds(pl.multiple_of((g * 2 + t) * width, width), width)
+
+    def slab(source, span):
+        start = pl.multiple_of(source * hidden_piece, 16)
+        return weights.at[:, pl.ds(start, hidden_piece), span]
+
+    def row_block(source, t):
+        start = pl.multiple_of((source * 2 + t) * row_count, row_count)
+        return rows.at[pl.ds(start, row_count)]
+
+    half = pl.ds(pl.multiple_of(gr * 2 * width, width), 2 * width)
+    far_half = pl.ds(pl.multiple_of((1 - gr) * 2 * width, width), 2 * width)
+
+    def piece_send(d, t):
+        return remote(
+            pieces_ref.at[d * 2 + t],
+            slab(fs, columns(gr, tp)),
+            piece_sem.at[d, t],
+            weight_sem.at[fs, tp],
+            (gr, d, t),
+        )
+
+    def column_send(source):
+        return remote(slab(source, half), slab(source, half), column_out_sem.at[source], column_sem.at[source], across)
+
+    def row_send(d):
+        return remote(rows_ref, row_block(fs, tp), row_out_sem.at[d], row_sem.at[fs], (gr, d, tp))
+
+    own_piece = pltpu.make_async_copy(
+        pieces_ref.at[expert], slab(fs, columns(gr, tp)), local_sem.at[0]
+    )
+    own_shared = pltpu.make_async_copy(
+        shared_ref, shared.at[:, :, columns(gr, tp)], local_sem.at[1]
+    )
+    own_rows = pltpu.make_async_copy(rows_ref, row_block(fs, tp), local_sem.at[2])
+    own_piece.start()
+    own_shared.start()
+    own_rows.start()
+
+    twin_piece = piece_send(fs, other)
+    twin_piece.start()
+    shared_far = remote(
+        shared_ref, shared.at[:, :, columns(gr, tp)], shared_out_sem.at[0], shared_sem.at[0], across
+    )
+    shared_far.start()
+    shared_twin = remote(
+        shared_ref, shared.at[:, :, columns(gr, tp)], shared_out_sem.at[1], shared_sem.at[1], twin
+    )
+    shared_twin.start()
+
+    for k in range(1, n):
+        d = lax.rem(fs + k, n)
+        piece_send(d, 0).start()
+        piece_send(d, 1).start()
+    for k in range(1, n):
+        row_send(lax.rem(fs + n - k, n)).start()
+    row_twin = remote(rows_ref, row_block(fs, tp), row_pair_out_sem.at[fs], row_pair_sem.at[fs], twin)
+    row_twin.start()
+
+    own_piece.wait()
+    twin_arrival = remote(
+        pieces_ref.at[0], slab(fs, columns(gr, other)), piece_sem.at[fs, other], weight_sem.at[fs, other], twin
+    )
+    twin_arrival.wait_recv()
+    column_send(fs).start()
+
+    for k in range(1, n):
+        source = lax.rem(fs + n - k, n)
+        for t in range(2):
+            remote(
+                pieces_ref.at[0],
+                slab(source, columns(gr, t)),
+                piece_sem.at[fs, other],
+                weight_sem.at[source, t],
+                twin,
+            ).wait_recv()
+        column_send(source).start()
+
+    own_shared.wait()
+    far_columns = shared.at[:, :, columns(1 - gr, tp)]
+    remote(shared_ref, far_columns, shared_out_sem.at[0], shared_sem.at[0], across).wait_recv()
+    shared_relay = remote(far_columns, far_columns, shared_out_sem.at[2], shared_sem.at[2], twin)
+    shared_relay.start()
+    remote(
+        shared_ref, shared.at[:, :, columns(gr, other)], shared_out_sem.at[1], shared_sem.at[1], twin
+    ).wait_recv()
+    last_columns = shared.at[:, :, columns(1 - gr, other)]
+    remote(shared_ref, last_columns, shared_out_sem.at[2], shared_sem.at[2], twin).wait_recv()
+    tail = pltpu.make_async_copy(
+        shared.at[:, pl.ds(pl.multiple_of(tp * extra, extra), extra), :],
+        weights.at[:, pl.ds(hidden, extra), :],
+        local_sem.at[3],
+    )
+    tail.start()
+
+    own_rows.wait()
+
+    def row_relay(source):
+        return remote(
+            row_block(source, tp),
+            row_block(source, tp),
+            row_pair_out_sem.at[source],
+            row_pair_sem.at[source],
+            twin,
+        )
+
+    for k in range(1, n):
+        source = lax.rem(fs + k, n)
+        remote(rows_ref, row_block(source, tp), row_out_sem.at[source], row_sem.at[source], twin).wait_recv()
+        row_relay(source).start()
+
+    for k in range(n):
+        source = lax.rem(fs + n - k, n)
+        remote(
+            slab(source, far_half),
+            slab(source, far_half),
+            column_out_sem.at[source],
+            column_sem.at[source],
+            across,
+        ).wait_recv()
+    tail.wait()
+    outs = []
+    for j, ref in enumerate((gate_ref, up_ref, down_ref)):
+        outs.append(
+            pltpu.make_async_copy(weights.at[j, pl.ds(0, hidden), :], ref.at[0], out_sem.at[j])
+        )
+    for j, ref in enumerate((shared_gate_ref, shared_up_ref, shared_down_ref)):
+        outs.append(pltpu.make_async_copy(shared.at[j], ref, out_sem.at[3 + j]))
+    for copy in outs:
+        copy.start()
+
+    def part_send(k):
+        return pltpu.make_async_remote_copy(
+            src_ref=parts.at[k, pl.ds(pl.multiple_of(other * row_count, row_count), row_count), :],
+            dst_ref=pair_in.at[k],
+            send_sem=part_sem.at[k],
+            recv_sem=part_recv_sem.at[k],
+            device_id=twin,
+            device_id_type=MESH,
+        )
+
+    def sum_send(k):
+        return pltpu.make_async_remote_copy(
+            src_ref=sums.at[k],
+            dst_ref=sums_in.at[k],
+            send_sem=sum_sem.at[k],
+            recv_sem=sum_recv_sem.at[k],
+            device_id=(gr, lax.rem(fs + 1 + k, n), tp),
+            device_id_type=MESH,
+        )
+
+    chunk = 32
+
+    def finish(k):
+        part_send(k).wait_recv()
+
+        @pl.loop(0, row_count // chunk)
+        def _(i):
+            at = pl.multiple_of(i * chunk, chunk)
+            mine = pl.multiple_of(tp * row_count + i * chunk, chunk)
+            value = parts[k, pl.ds(mine, chunk), :].astype(jnp.float32)
+            value = value + pair_in[k, pl.ds(at, chunk), :].astype(jnp.float32)
+            sums[k, pl.ds(at, chunk), :] = value.astype(jnp.bfloat16)
+
+    @pl.loop(0, n)
+    def _(k):
+        d = lax.rem(fs + 1 + k, n)
+        remote(
+            rows_ref, row_block(d, other), row_pair_out_sem.at[d], row_pair_sem.at[d], twin
+        ).wait_recv()
+        block = pl.ds(pl.multiple_of(d * 2 * row_count, 2 * row_count), 2 * row_count)
+        inputs = rows[block, 0:features]
+        factors = rows[block, features : features + LANES].astype(jnp.float32)
+        lane = lax.broadcasted_iota(jnp.int32, factors.shape, 1)
+        chosen = (lane == expert) | (lane == expert + LANES // 2)
+        factor = jnp.sum(jnp.where(chosen, factors, 0.0), axis=1, keepdims=True)
+        gate = contract_rows(inputs, weights[0])
+        up = contract_rows(inputs, weights[1])
+        unit = lax.broadcasted_iota(jnp.int32, gate.shape, 1)
+        scale = jnp.where(unit < hidden, factor, 1.0)
+        units = (gate / (1.0 + jnp.exp(-gate)) * up * scale).astype(jnp.bfloat16)
+        for c in range(4):
+            span = pl.ds(c * width, width)
+            parts[k, :, span] = jnp.dot(
+                units, weights[2, :, span], preferred_element_type=jnp.float32
+            ).astype(jnp.bfloat16)
+        part_send(k).start()
+
+        @pl.when(k > 0)
+        def _():
+            finish(k - 1)
+            sum_send(k - 1).start()
+
+    finish(n - 1)
+    for k in range(n - 1):
+        sum_send(k).wait_recv()
+
+    @pl.loop(0, row_count // chunk)
+    def _(i):
+        at = pl.ds(pl.multiple_of(i * chunk, chunk), chunk)
+        total = sums[n - 1, at, :].astype(jnp.float32)
+        for k in range(n - 1):
+            total = total + sums_in[k, at, :].astype(jnp.float32)
+        combined_ref[at, :] = total.astype(jnp.bfloat16)
+
+    twin_piece.wait_send()
+    shared_far.wait_send()
+    shared_twin.wait_send()
+    shared_relay.wait_send()
+    row_twin.wait_send()
+    column_send(fs).wait_send()
+    for k in range(1, n):
+        piece_send(lax.rem(fs + k, n), 0).wait_send()
+        piece_send(lax.rem(fs + k, n), 1).wait_send()
+        row_send(lax.rem(fs + k, n)).wait_send()
+        column_send(lax.rem(fs + k, n)).wait_send()
+        row_relay(lax.rem(fs + k, n)).wait_send()
+    for k in range(n):
+        part_send(k).wait_send()
+    for k in range(n - 1):
+        sum_send(k).wait_send()
+    for copy in outs:
+        copy.wait()
+
+
+def direct_body(
+    tokens,
+    routes,
+    route_weights,
+    norm_gain,
+    gate_trained,
+    up_trained,
+    down_trained,
+    shared_gate_trained,
+    shared_up_trained,
+    shared_down_trained,
+):
+    gain_row = norm_gain[None, None, :]
+    pieces = jnp.stack(
+        [gate_trained * gain_row, up_trained * gain_row, down_trained], axis=1
+    ).astype(jnp.bfloat16)
+    shared_gain = norm_gain[None, :]
+    shared_stack = jnp.stack(
+        [shared_gate_trained * shared_gain, shared_up_trained * shared_gain, shared_down_trained],
+        axis=0,
+    ).astype(jnp.bfloat16)
+    values = tokens.astype(jnp.float32)
+    normed = (
+        values * lax.rsqrt(jnp.mean(values * values, axis=1, keepdims=True) + epsilon)
+    ).astype(jnp.bfloat16)
+    n = lax.axis_size("fs")
+    experts, _, hidden_piece, width = pieces.shape
+    row_count, features = normed.shape
+    shared_piece = shared_stack.shape[1]
+    numbers = jnp.arange(LANES // 2, dtype=jnp.int32)
+    factors = jnp.sum(
+        jnp.where(routes[:, :, None] == numbers, route_weights[:, :, None], 0.0), axis=1
+    )
+    high = lax.reduce_precision(factors, 8, 7)
+    rows = jnp.concatenate(
+        [normed, high.astype(jnp.bfloat16), (factors - high).astype(jnp.bfloat16)], axis=1
+    )
+    hidden = n * hidden_piece
+    hidden_all = hidden + shared_piece // 2
+    vmem = pl.BlockSpec(memory_space=pltpu.VMEM)
+    hbm = pl.BlockSpec(memory_space=pl.ANY)
+    kind = jnp.bfloat16
+    expert_shape = jax.ShapeDtypeStruct((1, hidden, features), kind)
+    shared_shape = jax.ShapeDtypeStruct((shared_piece, features), kind)
+    DMA = pltpu.SemaphoreType.DMA
+    return pl.pallas_call(
+        functools.partial(exchange_kernel, n),
+        out_shape=(jax.ShapeDtypeStruct((row_count, features), kind),)
+        + (expert_shape,) * 3
+        + (shared_shape,) * 3,
+        in_specs=[vmem] * 3,
+        out_specs=(vmem,) + (hbm,) * 6,
+        scratch_shapes=[
+            pltpu.VMEM((3, hidden_all, features), kind),
+            pltpu.VMEM((3, shared_piece, features), kind),
+            pltpu.VMEM((experts * row_count, features + LANES), kind),
+            pltpu.VMEM((n, 2 * row_count, features), kind),
+            pltpu.VMEM((n, row_count, features), kind),
+            pltpu.VMEM((n, row_count, features), kind),
+            pltpu.VMEM((n - 1, row_count, features), kind),
+            DMA((4,)),
+            DMA((n, 2)),
+            DMA((n, 2)),
+            DMA((n,)),
+            DMA((n,)),
+            DMA((3,)),
+            DMA((3,)),
+            DMA((n,)),
+            DMA((n,)),
+            DMA((n,)),
+            DMA((n,)),
+            DMA((n,)),
+            DMA((n,)),
+            DMA((n - 1,)),
+            DMA((n - 1,)),
+            DMA((6,)),
+        ],
+        compiler_params=pltpu.CompilerParams(
+            collective_id=0, has_side_effects=True, vmem_limit_bytes=60 * 1024 * 1024
+        ),
+    )(pieces, shared_stack, rows)
+
+
+def body(*arguments):
+    experts = lax.axis_size("fs") * lax.axis_size("tp")
+    per_token = arguments[1].shape[1]
+    pairs = lax.axis_size("gr") == 2 and lax.axis_size("tp") == 2
+    if pairs and experts <= min(2 * per_token, LANES // 2):
+        return direct_body(*arguments)
+    return dispatch_body(*arguments)
+
+
 def solution(mesh):
     in_specs = (
         P(("gr", "fs", "tp"), None),

time: 507 us -> 298 us (0.59)
  waiting for transfers between devices: 350 us -> 0 us
  Pallas kernels: 0 us -> 278 us
  starting transfers between devices: 40.7 us -> 0 us
  local copies, waits for them, and re-layouts: 44.2 us -> 11.1 us
  matrix products: 24 us -> 0 us
  blocking collectives: 15.2 us -> 0 us
  between operations: 15.9 us -> 0.72 us
  other arithmetic: 16.8 us -> 8.23 us
    pallas_call x0 -> x1, Pallas kernels: none -> 278 us  [direct_body(): pl.pallas_call(functools.partial(exchange_kernel, n), out_shape=(jax.Shap...]
    all_gather x4 -> x0, waiting for transfers between devices: 268 us -> none  [the longest x1 111 us: body(): lax.all_gather(shared_gate, 'fs', axis=0, tiled=True)]
    all_to_all x3 -> x0, waiting for transfers between devices: 80.4 us -> none  [the longest x1 41.1 us: body(): lax.all_to_all(outgoing, ('fs', 'tp'), split_axis=0, concat_axis=0, tiled...]
    all_to_all x3 -> x0, starting transfers between devices: 40.3 us -> none  [the longest x1 28.2 us: body(): lax.all_to_all(result, ('fs', 'tp'), split_axis=0, concat_axis=0, tiled=T...]
    dot_general x4 -> x0, matrix products: 24 us -> none  [the longest x2 15.6 us: swiglu_rows(): return jnp.dot(hidden, down_matrix, preferred_element_type=jnp.float32)]
    gather x2 -> x0, local copies, waits for them, and re-layouts: 19.5 us -> none  [the longest x1 12.4 us: body(): returned.reshape(experts * capacity, features)[target].astype(jnp.float32)]
    all_gather x1 -> x0, blocking collectives: 8.72 us -> none  [body(): lax.all_gather(shared_stack, ('gr', 'tp'), axis=2, tiled=True)]
    all_gather x1 -> x0, local copies, waits for them, and re-layouts: 6.62 us -> none  [body(): owned = lax.all_gather(halves[:, :, :, None], 'gr', axis=3, tiled=True)]
  transfers between devices with their start and end apart: 7 -> 0, of which waited for: 7 -> 0; matrix products, arithmetic and copies ran while one was open for 11% -> 0% of each run, Pallas kernels for 0% -> 0%
where the time goes in v1:
time: 298 us
  Pallas kernels  278 us (93%)
  local copies, waits for them, and re-layouts  11.1 us (4%)
  other arithmetic  8.23 us (3%)
    pallas_call x1, Pallas kernels, direct_body(): pl.pallas_call(functools.partial(exchange_kernel, n), out_shape=(jax.Shap...  278 us
    unnamed x23, local copies, waits for them, and re-layouts  9.98 us

profile of v1, /device:TPU:0, one launch (start us, length us, event | category | flops | bytes accessed | tf_op | source)
XLA Modules:
  0.0 297.9 jit_solution(308456337569917085)
XLA Ops:
  0.6 0.0 copy-start
  0.6 1.3 fusion
  1.9 0.7 select_reduce_fusion
  2.7 0.1 copy.25
  2.8 0.1 copy.24
  2.9 0.0 copy-start.3
  2.9 0.0 copy-start.7
  2.9 1.2 fusion.4
  4.1 0.7 pad_maximum_fusion.1.shared_ref
  4.8 0.0 copy-done
  4.8 0.2 fusion.1
  5.0 0.9 concatenate.3.rows_ref
  6.0 0.0 copy-done.3
  6.0 0.0 copy-done.7
  6.0 2.5 fusion.2
  8.4 1.7 pad_maximum_fusion.pieces_ref
  10.1 277.9 %shard_map.153 = (bf16[128,2048]{1,0:T(8,128)(2,1)}, bf16[1,384,2048]{2,1,0:T(8,128)(2,1)}, bf16[1,384,2048]{2,1,0:T(8,128)(2,1)}, bf16[1,384,2048]{2,1,0:T(8,12...) custom-call(bf16[16,3,48,512]{3,2,1,0:T(8,128)(2,1)} %pad_maximum_fusion.pieces_ref, ...), custom_call_target="tpu_custom_call" | custom-call | tf_op jit(solution)/shard_map/pallas_call | solution.py:443
  288.0 1.9 copy.34
  289.8 0.0 copy-start.2
  289.8 2.8 copy.35
  292.7 0.0 copy-done.2
  292.7 0.0 copy-start.1
  292.7 1.1 copy.36
  293.8 0.8 copy-done.1
  294.7 0.0 copy-start.6
  294.7 0.0 copy-start.5
  294.7 0.0 copy-start.4
  294.7 1.1 copy.37
  295.8 0.0 copy-done.6
  295.8 0.7 copy.38
  296.5 0.0 copy-done.5
  296.5 0.7 copy.39
  297.2 0.0 copy-done.4
  297.2 0.7 copy.40
  (3 shorter events, 0.0 us)
Async XLA Ops:
  0.6 4.2 %copy-start = (bf16[128,2048]{1,0:T(8,128)(2,1)S(1)}, bf16[128,2048]{1,0:T(8,128)(2,1)}, u32[]{:S(2)}) copy-start(bf16[128,2048]{1,0:T(8,128)(2,1)} %param.10) | copy-start | bytes 1572868
  2.9 3.0 %copy-start.3 = (f32[16,48,512]{2,1,0:T(8,128)S(1)}, f32[16,48,512]{2,1,0:T(8,128)}, u32[]{:S(2)}) copy-start(f32[16,48,512]{2,1,0:T(8,128)} %param.14) | copy-start | bytes 4718596
  2.9 3.0 %copy-start.7 = (f32[512]{0:T(512)S(1)}, f32[512]{0:T(512)}, u32[]{:S(2)}) copy-start(f32[512]{0:T(512)} %param.13) | copy-start | bytes 6148
  289.8 2.9 copy-start.2
  292.7 2.0 copy-start.1
  294.7 1.2 copy-start.6
  294.7 1.9 copy-start.5
  294.7 2.6 copy-start.4

commit v2 on v1

--- a/solution.py
+++ b/solution.py
@@ -119,6 +119,7 @@
     parts,
     pair_in,
     sums,
+    side_in,
     sums_in,
     local_sem,
     piece_sem,
@@ -128,11 +129,15 @@
     shared_out_sem,
     shared_sem,
     row_out_sem,
+    row_side_sem,
+    row_back_sem,
     row_sem,
     row_pair_out_sem,
     row_pair_sem,
     part_sem,
     part_recv_sem,
+    side_sem,
+    side_recv_sem,
     sum_sem,
     sum_recv_sem,
     out_sem,
@@ -148,6 +153,9 @@
     extra = shared_piece // 2
     features = 4 * width
     row_count = rows_ref.shape[0]
+    depth = n // 2
+    outer, inner = lax.div(fs, 2), lax.rem(fs, 2)
+    beside = (gr, outer * 2 + 1 - inner, tp)
 
     barrier = pltpu.get_barrier_semaphore()
     pl.semaphore_signal(barrier, inc=1, device_id=across, device_id_type=MESH)
@@ -195,8 +203,39 @@
     def column_send(source):
         return remote(slab(source, half), slab(source, half), column_out_sem.at[source], column_sem.at[source], across)
 
-    def row_send(d):
-        return remote(rows_ref, row_block(fs, tp), row_out_sem.at[d], row_sem.at[fs], (gr, d, tp))
+    def row_move(source, send, recv, device):
+        return remote(row_block(source, tp), row_block(source, tp), send, recv, device)
+
+    def row_onward(source, step):
+        return row_move(
+            source,
+            row_out_sem.at[source],
+            row_sem.at[source],
+            (gr, (outer + step) * 2 + inner, tp),
+        )
+
+    def row_beside(source):
+        return row_move(source, row_side_sem.at[lax.div(source, 2)], row_sem.at[source], beside)
+
+    def row_relay(source):
+        return row_move(source, row_pair_out_sem.at[source], row_pair_sem.at[source], twin)
+
+    def row_back():
+        return row_move(
+            fs, row_back_sem.at[0], row_sem.at[fs], (gr, (outer - 1) * 2 + inner, tp)
+        )
+
+    def at_distance(action):
+        for distance in range(1, depth):
+            for step in (1, -1):
+                place = outer - step * distance
+
+                @pl.when((place >= 0) & (place < depth))
+                def _():
+                    action(place, step)
+
+    def onward_exists(step):
+        return (outer + step >= 0) & (outer + step < depth)
 
     own_piece = pltpu.make_async_copy(
         pieces_ref.at[expert], slab(fs, columns(gr, tp)), local_sem.at[0]
@@ -205,9 +244,21 @@
         shared_ref, shared.at[:, :, columns(gr, tp)], local_sem.at[1]
     )
     own_rows = pltpu.make_async_copy(rows_ref, row_block(fs, tp), local_sem.at[2])
+    own_rows.start()
     own_piece.start()
     own_shared.start()
-    own_rows.start()
+    own_rows.wait()
+
+    @pl.when(outer < depth - 1)
+    def _():
+        row_onward(fs, 1).start()
+
+    @pl.when(outer > 0)
+    def _():
+        row_back().start()
+
+    row_beside(fs).start()
+    row_relay(fs).start()
 
     twin_piece = piece_send(fs, other)
     twin_piece.start()
@@ -224,11 +275,6 @@
         d = lax.rem(fs + k, n)
         piece_send(d, 0).start()
         piece_send(d, 1).start()
-    for k in range(1, n):
-        row_send(lax.rem(fs + n - k, n)).start()
-    row_twin = remote(rows_ref, row_block(fs, tp), row_pair_out_sem.at[fs], row_pair_sem.at[fs], twin)
-    row_twin.start()
-
     own_piece.wait()
     twin_arrival = remote(
         pieces_ref.at[0], slab(fs, columns(gr, other)), piece_sem.at[fs, other], weight_sem.at[fs, other], twin
@@ -236,8 +282,10 @@
     twin_arrival.wait_recv()
     column_send(fs).start()
 
-    for k in range(1, n):
-        source = lax.rem(fs + n - k, n)
+    def take_rows(source):
+        row_move(source, row_out_sem.at[source], row_sem.at[source], twin).wait_recv()
+
+    def take_weights(source):
         for t in range(2):
             remote(
                 pieces_ref.at[0],
@@ -247,6 +295,29 @@
                 twin,
             ).wait_recv()
         column_send(source).start()
+
+    def arrive(place, step):
+        source = place * 2 + inner
+        take_rows(source)
+
+        @pl.when(onward_exists(step))
+        def _():
+            row_onward(source, step).start()
+
+        row_beside(source).start()
+        row_relay(source).start()
+        take_weights(source)
+        take_weights(place * 2 + 1 - inner)
+
+    def arrive_beside(place, step):
+        source = place * 2 + 1 - inner
+        take_rows(source)
+        row_relay(source).start()
+
+    take_weights(outer * 2 + 1 - inner)
+    at_distance(arrive)
+    arrive_beside(outer, 0)
+    at_distance(arrive_beside)
 
     own_shared.wait()
     far_columns = shared.at[:, :, columns(1 - gr, tp)]
@@ -265,22 +336,6 @@
     )
     tail.start()
 
-    own_rows.wait()
-
-    def row_relay(source):
-        return remote(
-            row_block(source, tp),
-            row_block(source, tp),
-            row_pair_out_sem.at[source],
-            row_pair_sem.at[source],
-            twin,
-        )
-
-    for k in range(1, n):
-        source = lax.rem(fs + k, n)
-        remote(rows_ref, row_block(source, tp), row_out_sem.at[source], row_sem.at[source], twin).wait_recv()
-        row_relay(source).start()
-
     for k in range(n):
         source = lax.rem(fs + n - k, n)
         remote(
@@ -311,19 +366,32 @@
             device_id_type=MESH,
         )
 
+    def place_of(k):
+        return lax.rem(outer + 1 + lax.rem(k, depth), depth)
+
+    def side_send(k):
+        return pltpu.make_async_remote_copy(
+            src_ref=sums.at[k],
+            dst_ref=side_in.at[k],
+            send_sem=side_sem.at[k],
+            recv_sem=side_recv_sem.at[k],
+            device_id=beside,
+            device_id_type=MESH,
+        )
+
     def sum_send(k):
         return pltpu.make_async_remote_copy(
             src_ref=sums.at[k],
-            dst_ref=sums_in.at[k],
-            send_sem=sum_sem.at[k],
-            recv_sem=sum_recv_sem.at[k],
-            device_id=(gr, lax.rem(fs + 1 + k, n), tp),
+            dst_ref=sums_in.at[k - depth],
+            send_sem=sum_sem.at[k - depth],
+            recv_sem=sum_recv_sem.at[k - depth],
+            device_id=(gr, place_of(k) * 2 + inner, tp),
             device_id_type=MESH,
         )
 
     chunk = 32
 
-    def finish(k):
+    def add_pair(k):
         part_send(k).wait_recv()
 
         @pl.loop(0, row_count // chunk)
@@ -334,11 +402,24 @@
             value = value + pair_in[k, pl.ds(at, chunk), :].astype(jnp.float32)
             sums[k, pl.ds(at, chunk), :] = value.astype(jnp.bfloat16)
 
+    def add_both(k):
+        part_send(k).wait_recv()
+        side_send(k - depth).wait_recv()
+
+        @pl.loop(0, row_count // chunk)
+        def _(i):
+            at = pl.multiple_of(i * chunk, chunk)
+            mine = pl.multiple_of(tp * row_count + i * chunk, chunk)
+            value = parts[k, pl.ds(mine, chunk), :].astype(jnp.float32)
+            value = value + pair_in[k, pl.ds(at, chunk), :].astype(jnp.float32)
+            value = value + side_in[k - depth, pl.ds(at, chunk), :].astype(jnp.float32)
+            sums[k, pl.ds(at, chunk), :] = value.astype(jnp.bfloat16)
+
     @pl.loop(0, n)
     def _(k):
-        d = lax.rem(fs + 1 + k, n)
+        d = place_of(k) * 2 + jnp.where(k < depth, 1 - inner, inner)
         remote(
-            rows_ref, row_block(d, other), row_pair_out_sem.at[d], row_pair_sem.at[d], twin
+            row_block(d, other), row_block(d, other), row_pair_out_sem.at[d], row_pair_sem.at[d], twin
         ).wait_recv()
         block = pl.ds(pl.multiple_of(d * 2 * row_count, 2 * row_count), 2 * row_count)
         inputs = rows[block, 0:features]
@@ -358,20 +439,25 @@
             ).astype(jnp.bfloat16)
         part_send(k).start()
 
-        @pl.when(k > 0)
+        @pl.when((k > 0) & (k <= depth))
         def _():
-            finish(k - 1)
+            add_pair(k - 1)
+            side_send(k - 1).start()
+
+        @pl.when(k > depth)
+        def _():
+            add_both(k - 1)
             sum_send(k - 1).start()
 
-    finish(n - 1)
-    for k in range(n - 1):
+    add_both(n - 1)
+    for k in range(depth, n - 1):
         sum_send(k).wait_recv()
 
     @pl.loop(0, row_count // chunk)
     def _(i):
         at = pl.ds(pl.multiple_of(i * chunk, chunk), chunk)
         total = sums[n - 1, at, :].astype(jnp.float32)
-        for k in range(n - 1):
+        for k in range(depth - 1):
             total = total + sums_in[k, at, :].astype(jnp.float32)
         combined_ref[at, :] = total.astype(jnp.bfloat16)
 
@@ -379,17 +465,38 @@
     shared_far.wait_send()
     shared_twin.wait_send()
     shared_relay.wait_send()
-    row_twin.wait_send()
+    row_relay(fs).wait_send()
+    row_beside(fs).wait_send()
+
+    @pl.when(outer < depth - 1)
+    def _():
+        row_onward(fs, 1).wait_send()
+
+    @pl.when(outer > 0)
+    def _():
+        row_back().wait_send()
+
+    def sent(place, step):
+        source = place * 2 + inner
+
+        @pl.when(onward_exists(step))
+        def _():
+            row_onward(source, step).wait_send()
+
+        row_beside(source).wait_send()
+
+    at_distance(sent)
     column_send(fs).wait_send()
     for k in range(1, n):
         piece_send(lax.rem(fs + k, n), 0).wait_send()
         piece_send(lax.rem(fs + k, n), 1).wait_send()
-        row_send(lax.rem(fs + k, n)).wait_send()
         column_send(lax.rem(fs + k, n)).wait_send()
         row_relay(lax.rem(fs + k, n)).wait_send()
     for k in range(n):
         part_send(k).wait_send()
-    for k in range(n - 1):
+    for k in range(depth):
+        side_send(k).wait_send()
+    for k in range(depth, n - 1):
         sum_send(k).wait_send()
     for copy in outs:
         copy.wait()
@@ -454,7 +561,8 @@
             pltpu.VMEM((n, 2 * row_count, features), kind),
             pltpu.VMEM((n, row_count, features), kind),
             pltpu.VMEM((n, row_count, features), kind),
-            pltpu.VMEM((n - 1, row_count, features), kind),
+            pltpu.VMEM((n // 2, row_count, features), kind),
+            pltpu.VMEM((n // 2 - 1, row_count, features), kind),
             DMA((4,)),
             DMA((n, 2)),
             DMA((n, 2)),
@@ -463,13 +571,17 @@
             DMA((3,)),
             DMA((3,)),
             DMA((n,)),
-            DMA((n,)),
-            DMA((n,)),
-            DMA((n,)),
-            DMA((n,)),
-            DMA((n,)),
-            DMA((n - 1,)),
-            DMA((n - 1,)),
+            DMA((n // 2,)),
+            DMA((1,)),
+            DMA((n,)),
+            DMA((n,)),
+            DMA((n,)),
+            DMA((n,)),
+            DMA((n,)),
+            DMA((n // 2,)),
+            DMA((n // 2,)),
+            DMA((n // 2 - 1,)),
+            DMA((n // 2 - 1,)),
             DMA((6,)),
         ],
         compiler_params=pltpu.CompilerParams(
@@ -482,7 +594,7 @@
     experts = lax.axis_size("fs") * lax.axis_size("tp")
     per_token = arguments[1].shape[1]
     pairs = lax.axis_size("gr") == 2 and lax.axis_size("tp") == 2
-    if pairs and experts <= min(2 * per_token, LANES // 2):
+    if pairs and lax.axis_size("fs") % 2 == 0 and experts <= min(2 * per_token, LANES // 2):
         return direct_body(*arguments)
     return dispatch_body(*arguments)
 

time: 298 us -> 196 us (0.66)
  the two profiles are of different devices: /device:TPU:0 before, /device:TPU:10 now
where the time goes in v2:
time: 196 us; the launch traced here: 195 us
  Pallas kernels  175 us (89%)
  local copies, waits for them, and re-layouts  11.1 us (6%)
  other arithmetic  8.23 us (4%)
    pallas_call x1, Pallas kernels, direct_body(): pl.pallas_call(functools.partial(exchange_kernel, n), out_shape=(jax.Shap...  175 us
    unnamed x23, local copies, waits for them, and re-layouts  9.98 us
    another operation x2, other arithmetic, direct_body(): jnp.stack([gate_trained * gain_row, up_trained * gain_row, down_trained],...  4.12 us

profile of v2, /device:TPU:10, one launch (start us, length us, event | category | flops | bytes accessed | tf_op | source)
XLA Modules:
  0.0 195.3 jit_solution(1399660088494963487)
XLA Ops:
  0.6 0.0 copy-start
  0.6 1.3 fusion
  1.9 0.7 select_reduce_fusion
  2.7 0.1 copy.25
  2.8 0.1 copy.24
  2.9 0.0 copy-start.3
  2.9 0.0 copy-start.7
  2.9 1.2 fusion.4
  4.1 0.7 pad_maximum_fusion.1.shared_ref
  4.8 0.0 copy-done
  4.8 0.2 fusion.1
  5.0 0.9 concatenate.3.rows_ref
  6.0 0.0 copy-done.3
  6.0 0.0 copy-done.7
  6.0 2.5 %fusion.2 = (bf16[16,1,48,512]{3,2,1,0:T(8,128)(2,1)S(1)}, bf16[16,1,48,512]{3,2,1,0:T(8,128)(2,1)S(1)}, bf16[16,1,48,512]{3,2,1,0:T(8,128)(2,1)S(1)}) fusion(f32[16,48,512]{2,1,0:T(8,128)S(1)} %copy-done.3, f32[512]{0:T(512)S(1)} %copy-done.7, f32[16,48,512]{2,1,0:T(8,128)} %param.15, f32[16,48,512]{2,1,0:T(8,128)} %param.16), kind=kLoop, calls=%fused_computation.7 | loop fusion | flops 1966080 | bytes 7079936 | tf_op jit(solution)/shard_map/stack | solution.py:518
  8.4 1.7 pad_maximum_fusion.pieces_ref
  10.1 175.3 %shard_map.153 = (bf16[128,2048]{1,0:T(8,128)(2,1)}, bf16[1,384,2048]{2,1,0:T(8,128)(2,1)}, bf16[1,384,2048]{2,1,0:T(8,128)(2,1)}, bf16[1,384,2048]{2,1,0:T(8,12...) custom-call(bf16[16,3,48,512]{3,2,1,0:T(8,128)(2,1)} %pad_maximum_fusion.pieces_ref, ...), custom_call_target="tpu_custom_call" | custom-call | tf_op jit(solution)/shard_map/pallas_call | solution.py:550
  185.4 1.9 copy.34
  187.3 0.0 copy-start.2
  187.3 2.8 %copy.35 = bf16[1,384,2048]{2,1,0:T(8,128)(2,1)} copy(bf16[1,384,2048]{2,1,0:T(8,128)(2,1)} %get-tuple-element.23) | data formatting | bytes 3145728
  190.1 0.0 copy-done.2
  190.1 0.0 copy-start.1
  190.1 1.1 copy.36
  191.3 0.8 copy-done.1
  192.1 0.0 copy-start.6
  192.1 0.0 copy-start.5
  192.1 0.0 copy-start.4
  192.1 1.1 copy.37
  193.2 0.0 copy-done.6
  193.2 0.7 copy.38
  193.9 0.0 copy-done.5
  193.9 0.7 copy.39
  194.6 0.0 copy-done.4
  194.6 0.7 copy.40
  (3 shorter events, 0.0 us)
Async XLA Ops:
  0.6 4.2 %copy-start = (bf16[128,2048]{1,0:T(8,128)(2,1)S(1)}, bf16[128,2048]{1,0:T(8,128)(2,1)}, u32[]{:S(2)}) copy-start(bf16[128,2048]{1,0:T(8,128)(2,1)} %param.10) | copy-start | bytes 1572868
  2.9 3.0 %copy-start.3 = (f32[16,48,512]{2,1,0:T(8,128)S(1)}, f32[16,48,512]{2,1,0:T(8,128)}, u32[]{:S(2)}) copy-start(f32[16,48,512]{2,1,0:T(8,128)} %param.14) | copy-start | bytes 4718596
  2.9 3.0 %copy-start.7 = (f32[512]{0:T(512)S(1)}, f32[512]{0:T(512)}, u32[]{:S(2)}) copy-start(f32[512]{0:T(512)} %param.13) | copy-start | bytes 6148
  187.3 2.9 %copy-start.2 = (bf16[1,384,2048]{2,1,0:T(8,128)(2,1)S(1)}, bf16[1,384,2048]{2,1,0:T(8,128)(2,1)}, u32[]{:S(2)}) copy-start(bf16[1,384,2048]{2,1,0:T(8,128)(2,1)} %get-tuple-element.24) | copy-start | bytes 4718596
  190.1 2.0 %copy-start.1 = (bf16[1,384,2048]{2,1,0:T(8,128)(2,1)S(1)}, bf16[1,384,2048]{2,1,0:T(8,128)(2,1)}, u32[]{:S(2)}) copy-start(bf16[1,384,2048]{2,1,0:T(8,128)(2,1)} %get-tuple-element.25) | copy-start | bytes 4718596
  192.1 1.2 copy-start.6
  192.1 1.9 copy-start.5
  192.1 2.6 %copy-start.4 = (bf16[64,2048]{1,0:T(8,128)(2,1)S(1)}, bf16[64,2048]{1,0:T(8,128)(2,1)}, u32[]{:S(2)}) copy-start(bf16[64,2048]{1,0:T(8,128)(2,1)} %get-tuple-element.28) | copy-start | bytes 786436
